TPU v7x, 1024 devices: a whole 4x8x16 slice. The times are simulated.
1024 devices in a mesh: ep: 32 (over z, core), tp: 32 (over y, x).
Axes of the slice: x: 4, y: 8, z: 16, core: 2. Of those that a mesh axis runs over, the one named last changes fastest.
Arguments:
- tokens: bfloat16 [4096, 4096], P('ep', 'tp'), may hold values from -6 to 6
- routes: int32 [4096, 2], P('ep'), may hold values from 0 to 63, all different within a row; in each aligned block of 128 rows (0 to 127, 128 to 255, ...) at most 5 rows name the same one
- route_weights: float32 [4096, 2], P('ep'), may hold values from 0.2 to 2
- cotangent: bfloat16 [4096, 4096], P('ep', 'tp'), may hold values from -6 to 6
- expert_gate: bfloat16 [64, 4096, 512], P('ep', 'tp'), may hold values from -0.09375 to 0.09375
- expert_up: bfloat16 [64, 4096, 512], P('ep', 'tp'), may hold values from -0.09375 to 0.09375
- expert_down: bfloat16 [64, 512, 4096], P('ep', None, 'tp'), may hold values from -0.25 to 0.25
- shared_gate: bfloat16 [4096, 512], P('tp'), may hold values from -0.09375 to 0.09375
- shared_up: bfloat16 [4096, 512], P('tp'), may hold values from -0.09375 to 0.09375
- shared_down: bfloat16 [512, 4096], P(None, 'tp'), may hold values from -0.25 to 0.25
Outputs:
- grad_tokens: bfloat16 [4096, 4096], P('ep', 'tp')
- grad_weights: float32 [4096, 2], P('ep')
- grad_expert_gate: float32 [64, 4096, 512], P('ep', 'tp')
- grad_expert_up: float32 [64, 4096, 512], P('ep', 'tp')
- grad_expert_down: float32 [64, 512, 4096], P('ep', None, 'tp')
- grad_shared_gate: float32 [4096, 512], P('tp', 'ep')
- grad_shared_up: float32 [4096, 512], P('tp', 'ep')
- grad_shared_down: float32 [512, 4096], P('ep', 'tp')
Inputs may be any that keep to these rules, and one draw needn't show every extreme that they name: `routes`: each row names 2 different experts. In each aligned block of 128 rows (the rows of one index of ep) no expert is named by more than 5 rows, a bound that some block reaches.
All inputs are finite; a program needn't handle non-finite values.
Results may differ from a plain program's by a relative error of at most 0.0054.
Values may be sent and summed in bfloat16 or wider, within the bound.
No kernel may reach another device: no remote copies, remote signals or barrier semaphores. Data moves between devices by JAX's collectives and lax.ppermute only.
A program may use at most 32 MiB of HBM per device.

v0:
```python
import jax
import jax.numpy as jnp
from jax import lax
from jax.experimental import pallas as pl
from jax.experimental.pallas import tpu as pltpu
from jax.sharding import Mesh
from jax.sharding import PartitionSpec as P

BF, F16, F32, I32 = jnp.bfloat16, jnp.float16, jnp.float32, jnp.int32
NZ, NC, NY, NX = 16, 2, 8, 4
NEP, NTP = NZ * NC, NY * NX
CAP, BLK = 5, 16
SLOTS = 2 * CAP
SHR = 4
USED = SLOTS + SHR
HID = 512
SCALE_X, SCALE_Y = 256.0, 64.0

SHIFTS = (1, 3, 2)


def iota(shape, dim):
    return lax.broadcasted_iota(I32, shape, dim)


def nn(a, b):
    return jnp.dot(a, b, preferred_element_type=F32)


def nt(a, b):
    return lax.dot_general(a, b, (((1,), (1,)), ((), ())), preferred_element_type=F32)


def tn(a, b):
    return lax.dot_general(a, b, (((0,), (0,)), ((), ())), preferred_element_type=F32)


def onehot(cond):
    return jnp.where(cond, 1.0, 0.0).astype(BF)


def call(kernel, outs, space=pltpu.VMEM, scratch=()):
    def place(o):
        return o if isinstance(o, jax.ShapeDtypeStruct) else pltpu.VMEM(*o)

    outs = [place(o) for o in outs]

    def run(*args):
        return pl.pallas_call(
            kernel,
            out_shape=outs,
            in_specs=[pl.BlockSpec(memory_space=space)] * len(args),
            out_specs=[pl.BlockSpec(memory_space=pltpu.VMEM)] * len(outs),
            scratch_shapes=scratch,
            compiler_params=pltpu.CompilerParams(vmem_limit_bytes=16 << 20),
        )(*[pltpu.with_memory_space_constraint(a, space) for a in args])

    return run


def struct(shape, dtype):
    return jax.ShapeDtypeStruct(shape, dtype)


def route_kernel(*refs):
    sources, (send, ids), kept = refs[:10], refs[10:12], refs[12:20]
    routes, weights, sems = refs[20:]
    tok, cot = kept[:2]
    copies = [
        pltpu.make_async_copy(a, b, sems.at[k])
        for k, (a, b) in enumerate(zip(sources, (routes, weights, *kept)))
    ]
    for copy in copies:
        copy.start()
    for copy in copies[:4]:
        copy.wait()
    n = tok.shape[0]
    r0, r1 = routes[0:1, :], routes[1:2, :]
    names = iota((NEP * 2, n), 0)
    f0, f1 = jnp.where(r0 == names, 1.0, 0.0), jnp.where(r1 == names, 1.0, 0.0)
    earlier = onehot(iota((n, n), 0) < iota((n, n), 1))
    c0 = nn(f0.astype(BF), earlier)
    c1 = nn(f1.astype(BF), earlier) + jnp.sum(f0, axis=1, keepdims=True)
    rank0 = jnp.sum(c0 * f0, axis=0, keepdims=True).astype(I32)
    rank1 = jnp.sum(c1 * f1, axis=0, keepdims=True).astype(I32)
    row0 = (r0 >> 1) * BLK + (r0 & 1) * CAP + rank0
    row1 = (r1 >> 1) * BLK + (r1 & 1) * CAP + rank1
    ids[0:1, :] = row0
    ids[1:2, :] = row1
    tall = iota((NEP * BLK, n), 0)
    places = onehot((row0 == tall) | (row1 == tall))
    send[:, 128:] = nn(places, cot[...]).astype(BF)
    gates = weights[...].astype(BF).astype(F32)
    data = nn(places, tok[...])
    lane = iota((n, n), 0)
    for row, k in ((row0, 0), (row1, 1)):
        at = jnp.where((row >> 4) * BLK + SLOTS == tall, gates[k : k + 1, :], 0.0).astype(BF)
        data = data + nt(at, onehot(lane == (row & 15)))
    send[:, :128] = data.astype(BF)
    for copy in copies[4:]:
        copy.wait()


def split_rows(r, size):
    if size == USED:
        x = (r * 293) >> 15
        rest = r - x * (NY * USED)
        y = (rest * 293) >> 12
    else:
        x = (r * 205) >> 14
        rest = r - x * (NY * SLOTS)
        y = (rest * 205) >> 11
    return x, y, rest - y * size


def shared_kernel(tok, cot, sg, su, sd, *outs):
    me = lax.axis_index("x")
    r = iota((NTP * SHR, 1), 0)
    s = ((r >> 2) & (NY - 1)) * NX + (((r >> 5) + me) & (NX - 1))
    pick = onehot(s * SHR + (r & 3) == iota((NTP * SHR, 128), 1))
    t = nn(pick, tok[...]).astype(BF)
    c = nn(pick, cot[...]).astype(BF)
    rows = NY * SHR
    for j, part in enumerate((nn(t, sg[...]), nn(t, su[...]), nt(c, sd[...]))):
        for k in range(NX):
            outs[k][:, j * HID : j * HID + HID] = part[k * rows : k * rows + rows] * SCALE_X


def partial_kernel(recv, wg, wu, wd, out):
    x, y, q = split_rows(iota((NTP * SLOTS, 1), 0), SLOTS)
    pick = onehot((y * NX + x) * BLK + q == iota((NTP * SLOTS, NEP * BLK), 1))
    data = nn(pick, recv[...])
    t, c = data[:, :128], data[:, 128:]
    kinds = (q < CAP, q >= CAP)
    tcat = jnp.concatenate([jnp.where(k, t, 0.0).astype(BF) for k in kinds], axis=1)
    ccat = jnp.concatenate([jnp.where(k, c, 0.0).astype(BF) for k in kinds], axis=1)
    wgc = jnp.concatenate([wg[0], wg[1]], axis=0)
    wuc = jnp.concatenate([wu[0], wu[1]], axis=0)
    wdc = jnp.concatenate([wd[0], wd[1]], axis=1)
    out[:, :HID] = nn(tcat, wgc) * SCALE_X
    out[:, HID : 2 * HID] = nn(tcat, wuc) * SCALE_X
    out[:, 2 * HID :] = nt(ccat, wdc) * SCALE_X


def merge_kernel(routed, shared, out):
    for y in range(NY):
        at = y * BLK
        out[at : at + SLOTS] = routed[y * SLOTS : y * SLOTS + SLOTS] * (SCALE_Y / SCALE_X)
        out[at + SLOTS : at + USED] = shared[y * SHR : y * SHR + SHR] * (SCALE_Y / SCALE_X)
        out[at + USED : at + BLK] = jnp.zeros((BLK - USED, out.shape[1]), F32)


def hidden_kernel(got, recv, out):
    t = lax.axis_index("y") * NX + lax.axis_index("x")
    pre = got[...] * (1.0 / SCALE_Y)
    gate, up, back = pre[:, :HID], pre[:, HID : 2 * HID], pre[:, 2 * HID :]
    q = iota((BLK, 1), 0)
    lane = iota((BLK, 128), 1)
    block = recv[t, :, :128].astype(F32)
    grow = jnp.sum(jnp.where(iota((BLK, 128), 0) == SLOTS, block, 0.0), axis=0, keepdims=True)
    gcol = jnp.sum(jnp.where(lane == iota((BLK, 128), 0), grow, 0.0), axis=1, keepdims=True)
    scale = jnp.where(q < SLOTS, gcol, 1.0)
    logistic = jax.nn.sigmoid(gate)
    product = gate * logistic * up
    grad_act = scale * back
    gate_grad = (grad_act * up * logistic * (1.0 + gate * (1.0 - logistic))).astype(BF)
    up_grad = (grad_act * gate * logistic).astype(BF)
    hidden = (scale * product).astype(BF)
    dg = jnp.sum(back * product, axis=1, keepdims=True)
    lane_h = iota((BLK, HID), 1)
    row_h = iota((BLK, HID), 0)
    line = jnp.sum(jnp.where(lane_h == row_h, dg, 0.0), axis=0, keepdims=True)
    high = line.astype(BF).astype(F32)
    extra = jnp.where(row_h == USED, high, line - high)
    gate_grad = jnp.where(row_h >= USED, extra, gate_grad.astype(F32)).astype(BF)
    for k in range(NY):
        out[k, :, :HID] = gate_grad
        out[k, :, HID : 2 * HID] = up_grad
        out[k, :, 2 * HID :] = hidden


def pack_kernel(own, main, hid):
    data = own[:, : 2 * HID]
    hidden = own[:, 2 * HID :]
    r = iota((NY * USED, 1), 0)
    _, y, q = split_rows(r, USED)
    grads = nn(onehot(y * BLK + q == iota((NY * USED, NY * BLK), 1)), data).astype(BF)
    j = iota((BLK, 1), 0)
    lane = iota((BLK, NY * BLK), 1)
    left = nn(onehot((j >> 2) * BLK + SLOTS + (j & 3) == lane), hidden)
    right = nn(onehot(((j >> 2) + 4) * BLK + SLOTS + (j & 3) == lane), hidden)
    row = iota((NY, 1), 0) * BLK + USED
    lane = iota((NY, NY * BLK), 1)
    high = nn(onehot(row == lane), data[:, :128])
    low = nn(onehot(row + 1 == lane), data[:, :128])
    rest = jnp.zeros((NY, 2 * HID - 256), F32)
    shared = jnp.concatenate([left, right], axis=1).astype(BF)
    lines = jnp.concatenate([high, low, rest], axis=1).astype(BF)
    for k in range(NX):
        main[k, : NY * USED] = grads
        main[k, NY * USED : NY * BLK] = shared
        main[k, NY * BLK :] = lines
    _, y, q = split_rows(iota((NY * SLOTS, 1), 0), SLOTS)
    hid[...] = nn(onehot(y * BLK + q == iota((NY * SLOTS, NY * BLK), 1)), hidden).astype(BF)


def back_kernel(main, tok, cot, wg, wu, sg, su, shared_grad, send):
    n = tok.shape[0]
    rows, total = NY * USED, NTP * USED
    grads = jnp.concatenate([main[x, :rows] for x in range(NX)], axis=0)
    hidden = jnp.concatenate([main[x, rows : NY * BLK] for x in range(NX)], axis=0)
    lines = jnp.concatenate([main[x, NY * BLK :, :256] for x in range(NX)], axis=0)
    token = iota((n, 1), 0)
    y, x, t = token >> 4, (token >> 2) & 3, token & 3
    pick = onehot(x * rows + y * USED + SLOTS + t == iota((n, total), 1))
    shared = nn(pick, grads).astype(BF)
    j = y * SHR + t
    place = x * BLK + (j & 15)
    lane = iota((n, NX * BLK), 1)
    near = onehot((j < BLK) & (place == lane))
    far = onehot((j >= BLK) & (place == lane))
    shared_hidden = (nn(near, hidden[:, :HID]) + nn(far, hidden[:, HID:])).astype(BF)
    shared_grad[...] = nt(shared[:, :HID], sg[...]) + nt(shared[:, HID:], su[...])
    wt = tn(shared, tok[...]).astype(BF)
    wdn = tn(shared_hidden, cot[...]).astype(BF)
    gg, gu = grads[:, :HID], grads[:, HID:]
    d0 = nt(gg, wg[0]) + nt(gu, wu[0])
    d1 = nt(gg, wg[1]) + nt(gu, wu[1])
    _, _, q = split_rows(iota((total, 1), 0), USED)
    slots = jnp.where(q < CAP, d0, d1).astype(BF)
    o = iota((NEP * BLK, 1), 0)
    q, d = o & 15, o >> 4
    want = jnp.where(q < SLOTS, (d & 3) * rows + (d >> 2) * USED + q, -1)
    back = nn(onehot(want == iota((NEP * BLK, total), 1)), slots)
    source = (d & 3) * NY + (d >> 2)
    lane = iota((NEP * BLK, NTP), 1)
    back = back + nn(onehot((q == USED) & (source == lane)), lines[:, :128])
    back = back + nn(onehot((q == USED + 1) & (source == lane)), lines[:, 128:])
    back = back.astype(BF)
    for d in range(NEP):
        z, c = d // NC, d % NC
        send[c, z, 0:BLK] = back[d * BLK : d * BLK + BLK]
        send[c, z, BLK : 2 * BLK] = wt[d * BLK : d * BLK + BLK]
        send[c, z, 2 * BLK : 3 * BLK] = wt[HID + d * BLK : HID + d * BLK + BLK]
        send[c, z, 3 * BLK :] = wdn[d * BLK : d * BLK + BLK]


def weights_kernel(main, recv, og, ou):
    rows, total = NY * USED, NTP * USED
    grads = jnp.concatenate([main[x, :rows] for x in range(NX)], axis=0)
    x, y, q = split_rows(iota((total, 1), 0), USED)
    place = (y * NX + x) * BLK + q
    lane = iota((total, NEP * BLK), 1)
    data = recv[:, :128]
    t0 = nn(onehot((q < CAP) & (place == lane)), data).astype(BF)
    t1 = nn(onehot((q >= CAP) & (q < SLOTS) & (place == lane)), data).astype(BF)
    tcat = jnp.concatenate([t0, t1], axis=1)
    g = tn(tcat, grads[:, :HID])
    og[0], og[1] = g[:128], g[128:]
    u = tn(tcat, grads[:, HID:])
    ou[0], ou[1] = u[:128], u[128:]


def down_kernel(h0, h1, h2, h3, recv, od):
    me = lax.axis_index("x")
    hidden = jnp.concatenate([h0[...], h1[...], h2[...], h3[...]], axis=0)
    k, y, q = split_rows(iota((NTP * SLOTS, 1), 0), SLOTS)
    place = (y * NX + ((me - k) & (NX - 1))) * BLK + q
    lane = iota((NTP * SLOTS, NEP * BLK), 1)
    data = recv[:, 128:]
    c0 = nn(onehot((q < CAP) & (place == lane)), data).astype(BF)
    c1 = nn(onehot((q >= CAP) & (place == lane)), data).astype(BF)
    d = tn(hidden, jnp.concatenate([c0, c1], axis=1))
    od[0], od[1] = d[:, :128], d[:, 128:]


def core_kernel(got, out):
    for z in range(NZ):
        out[z, :BLK] = got[0, z, :BLK]
        out[z, BLK : 2 * BLK] = got[1, z, :BLK]
        both = got[0, z, BLK:].astype(F32) + got[1, z, BLK:].astype(F32)
        out[z, 2 * BLK :] = both.astype(BF)


def final_kernel(got, ids, shared_grad, grad_tokens, grad_weights, og, ou, od):
    n = ids.shape[1]
    row0, row1 = ids[0:1, :], ids[1:2, :]
    back = jnp.concatenate([got[z, : 2 * BLK] for z in range(NZ)], axis=0)
    tall = iota((NEP * BLK, n), 0)
    places = onehot((row0 == tall) | (row1 == tall))
    grad_tokens[...] = (tn(places, back) + shared_grad[...]).astype(BF)
    lane = iota((n, n), 0)
    for row, k in ((row0, 0), (row1, 1)):
        base = (row >> 4) * BLK + USED
        line = tn(back, onehot((tall == base) | (tall == base + 1)))
        grad_weights[k : k + 1, :] = jnp.sum(
            jnp.where(lane == (row & 15), line, 0.0), axis=0, keepdims=True
        )
    total = got[0, 2 * BLK :].astype(F32)
    for z in range(1, NZ):
        total = total + got[z, 2 * BLK :].astype(F32)
    og[...] = total[:BLK]
    ou[...] = total[BLK : 2 * BLK]
    od[...] = total[2 * BLK :]


def swap(array, axis):
    return lax.all_to_all(array, axis, 0, 0, tiled=True)


def turn(array, shift):
    return lax.ppermute(array, "x", [(i, (i + shift) % NX) for i in range(NX)])


def body(tok, routes, weights, cot, wg, wu, wd, sg, su, sd):
    n, feats = tok.shape
    wide = 3 * HID
    params = (tok, cot, wg, wu, wd, sg, su, sd)
    send, ids, *params = call(
        route_kernel,
        [((NEP * BLK, 2 * feats), BF), ((2, n), I32)] + [(p.shape, BF) for p in params],
        space=pltpu.HBM,
        scratch=[
            pltpu.VMEM((2, n), I32),
            pltpu.VMEM((2, n), F32),
            pltpu.SemaphoreType.DMA((10,)),
        ],
    )(routes.T, weights.T, *params)
    tok, cot, wg, wu, wd, sg, su, sd = params
    recv = swap(send.reshape(NEP, BLK, 2 * feats), ("z", "core"))
    shared = call(shared_kernel, [((NY * SHR, wide), F32)] * NX)(tok, cot, sg, su, sd)
    moved = [turn(shared[k].astype(F16), k).astype(F32) for k in SHIFTS]
    shared = sum(moved, shared[0])
    recv, shared = lax.optimization_barrier((recv, shared))
    flat = recv.reshape(NEP * BLK, 2 * feats)
    (part,) = call(partial_kernel, [((NTP * SLOTS, wide), F32)])(flat, wg, wu, wd)
    got = swap(part.astype(F16).reshape(NX, NY * SLOTS, wide), "x")
    routed = jnp.sum(got.astype(F32), axis=0)
    (mid,) = call(merge_kernel, [((NY * BLK, wide), F32)])(routed, shared)
    got = swap(mid.astype(F16).reshape(NY, BLK, wide), "y")
    pre = jnp.sum(got.astype(F32), axis=0)
    (grads,) = call(hidden_kernel, [((NY, BLK, wide), BF)])(pre, recv)
    own = swap(grads, "y").reshape(NY * BLK, wide)
    main, hid = call(
        pack_kernel, [((NX, NY * (BLK + 1), 2 * HID), BF), ((NY * SLOTS, HID), BF)]
    )(own)
    main = swap(main, "x")
    shared_grad, back = call(
        back_kernel, [((n, feats), F32), ((NC, NZ, 4 * BLK, feats), BF)]
    )(main, tok, cot, wg, wu, sg, su)
    back = swap(back, "core")
    (back,) = call(core_kernel, [((NZ, 5 * BLK, feats), BF)])(back)
    hid, back = lax.optimization_barrier((hid, back))
    turned = {k: turn(hid, k) for k in SHIFTS}
    back = swap(back, "z")
    grad_g, grad_u = call(
        weights_kernel, [struct((2, feats, HID), F32), struct((2, feats, HID), F32)]
    )(main, flat)
    (grad_d,) = call(down_kernel, [struct((2, HID, feats), F32)])(
        hid, turned[1], turned[2], turned[3], flat
    )
    grad_tokens, grad_weights, shared_g, shared_u, shared_d = call(
        final_kernel,
        [
            struct((n, feats), BF),
            struct((2, n), F32),
            struct((BLK, feats), F32),
            struct((BLK, feats), F32),
            struct((BLK, feats), F32),
        ],
    )(back, ids, shared_grad)
    return grad_tokens, grad_weights.T, grad_g, grad_u, grad_d, shared_g.T, shared_u.T, shared_d


def solution(mesh):
    return program(mesh)


def program(mesh):
    ep, tp = ("z", "core"), ("y", "x")
    fine = Mesh(mesh.devices.reshape(NZ, NC, NY, NX), ("z", "core", "y", "x"))
    return jax.shard_map(
        body,
        mesh=fine,
        in_specs=(
            P(ep, tp),
            P(ep, None),
            P(ep, None),
            P(ep, tp),
            P(ep, tp, None),
            P(ep, tp, None),
            P(ep, None, tp),
            P(tp, None),
            P(tp, None),
            P(None, tp),
        ),
        out_specs=(
            P(ep, tp),
            P(ep, None),
            P(ep, tp, None),
            P(ep, tp, None),
            P(ep, None, tp),
            P(tp, ep),
            P(tp, ep),
            P(ep, tp),
        ),
        check_vma=False,
    )
```

profile of v0, /device:TPU:2, one launch (start us, length us, event | category | flops | bytes accessed | tf_op | source)
XLA Modules:
  0.0 148.5 jit_solution(16404144608679379764)
XLA Ops:
  0.6 2.1 %shard_map.161 = (bf16[512,256]{1,0:T(8,128)(2,1)}, s32[2,128]{1,0:T(2,128)S(1)}, bf16[128,128]{1,0:T(8,128)(2,1)S(1)}, bf16[128,128]{1,0:T(8,128)(2,1)S(1)}, bf...) custom-call(s32[2,128]{1,0:T(2,128)} %bitcast.16, ...), custom_call_target="tpu_custom_call" | custom-call | tf_op jit(solution)/shard_map/pallas_call | solution.py:49
  2.8 19.2 %all-to-all-start = ((bf16[32,16,256]{2,1,0:T(8,128)(2,1)}), bf16[32,16,256]{2,1,0:T(8,128)(2,1)S(1)}, u32[]{:S(2)}, u32[]{:S(2)}) async-start(bf16[32,16,256]{2,1,0:T(8,128)(2,1)} %bitcast.2), calls=%async_computation | async-start | bytes 524288 | tf_op jit(solution)/shard_map/all_to_all | solution.py:308
  22.3 4.0 %collective-permute-start.2 = (f16[32,1536]{1,0:T(8,128)(2,1)S(1)}, f16[32,1536]{1,0:T(8,128)(2,1)S(1)}, u32[]{:S(2)}, u32[]{:S(2)}) collective-permute-start(f16[32,1536]{1,0:T(8,128)(2,1)S(1)} %convert_element_type.34), channel_id=1, source_target_pairs={{0,2},{1,3},{2,0},{3,1},{4,6},{5,7},{6,4},{7,5},{8,10},{9,11},{10,... | collective-permute-start | bytes 294920 | tf_op jit(solution)/shard_map/ppermute | solution.py:312
  26.4 3.4 %collective-permute-start.1 = (f16[32,1536]{1,0:T(8,128)(2,1)S(1)}, f16[32,1536]{1,0:T(8,128)(2,1)S(1)}, u32[]{:S(2)}, u32[]{:S(2)}) collective-permute-start(f16[32,1536]{1,0:T(8,128)(2,1)S(1)} %convert_element_type.32), channel_id=1, source_target_pairs={{0,3},{1,0},{2,1},{3,2},{4,7},{5,4},{6,5},{7,6},{8,11},{9,8},{10,9... | collective-permute-start | bytes 294920 | tf_op jit(solution)/shard_map/ppermute | solution.py:312
  29.8 2.5 %collective-permute-start = (f16[32,1536]{1,0:T(8,128)(2,1)S(1)}, f16[32,1536]{1,0:T(8,128)(2,1)S(1)}, u32[]{:S(2)}, u32[]{:S(2)}) collective-permute-start(f16[32,1536]{1,0:T(8,128)(2,1)S(1)} %convert_element_type.30), channel_id=1, source_target_pairs={{0,1},{1,2},{2,3},{3,0},{4,5},{5,6},{6,7},{7,4},{8,9},{9,10},{10,1... | collective-permute-start | bytes 294920 | tf_op jit(solution)/shard_map/ppermute | solution.py:312
  32.3 0.7 collective-permute-done.1
  33.0 3.3 %collective-permute-done = f16[32,1536]{1,0:T(8,128)(2,1)S(1)} collective-permute-done((f16[32,1536]{1,0:T(8,128)(2,1)S(1)}, f16[32,1536]{1,0:T(8,128)(2,1)S(1)}, u32[]{:S(2)}, u32[]{:S(2)}) %collective-permute-start) | collective-permute-done | bytes 98336 | tf_op jit(solution)/shard_map/ppermute | solution.py:312
  36.3 8.3 %all-to-all-done.recv = bf16[32,16,256]{2,1,0:T(8,128)(2,1)S(1)} async-done(((bf16[32,16,256]{2,1,0:T(8,128)(2,1)}), bf16[32,16,256]{2,1,0:T(8,128)(2,1)S(1)}, u32[]{:S(2)}, u32[]{:S(2)}) %all-to-all-start) | async-done | bytes 262176 | tf_op jit(solution)/shard_map/all_to_all | solution.py:308
  44.6 0.7 shard_map.163
  45.4 17.6 %all_to_all.35 = f16[4,80,1536]{2,1,0:T(8,128)(2,1)S(1)} all-to-all(f16[4,80,1536]{2,1,0:T(8,128)(2,1)S(1)} %bitcast.14), channel_id=1, replica_groups=mesh['z'=16,'core'=2,'y'=8,'x'=4] {'x'}, dimensions={0} | all-to-all | bytes 1966080 | tf_op jit(solution)/shard_map/all_to_all | solution.py:308
  63.4 20.5 %all_to_all.36 = f16[8,16,1536]{2,1,0:T(8,128)(2,1)S(1)} all-to-all(f16[8,16,1536]{2,1,0:T(8,128)(2,1)S(1)} %bitcast.15), channel_id=1, replica_groups=mesh['z'=16,'core'=2,'y'=8,'x'=4] {'y'}, dimensions={0} | all-to-all | bytes 786432 | tf_op jit(solution)/shard_map/all_to_all | solution.py:308
  84.0 15.5 %all_to_all.37 = bf16[8,16,1536]{2,1,0:T(8,128)(2,1)S(1)} all-to-all(bf16[8,16,1536]{2,1,0:T(8,128)(2,1)S(1)} %shard_map.165), channel_id=1, replica_groups=mesh['z'=16,'core'=2,'y'=8,'x'=4] {'y'}, dimensions={0} | all-to-all | bytes 786432 | tf_op jit(solution)/shard_map/all_to_all | solution.py:308
  99.9 15.1 %all_to_all.38.main = bf16[4,136,1024]{2,1,0:T(8,128)(2,1)S(1)} all-to-all(bf16[4,136,1024]{2,1,0:T(8,128)(2,1)S(1)} %get-tuple-element.53), channel_id=1, replica_groups=mesh['z'=16,'core'=2,'y'=8,'x'=4] {'x'}, dimensions={0} | all-to-all | bytes 2228224 | tf_op jit(solution)/shard_map/all_to_all | solution.py:308
  115.0 1.4 shard_map.167
  116.4 4.2 %all_to_all.39.got = bf16[2,16,64,128]{3,2,1,0:T(8,128)(2,1)S(1)} all-to-all(bf16[2,16,64,128]{3,2,1,0:T(8,128)(2,1)S(1)} %get-tuple-element.54), channel_id=1, replica_groups=mesh['z'=16,'core'=2,'y'=8,'x'=4] {'core'}, dimensions={0} | all-to-all | bytes 1048576 | tf_op jit(solution)/shard_map/all_to_all | solution.py:308
  120.6 0.8 shard_map.168
  121.3 4.9 %all-to-all-start.6 = ((bf16[16,80,128]{2,1,0:T(8,128)(2,1)}), bf16[16,80,128]{2,1,0:T(8,128)(2,1)S(1)}, u32[]{:S(2)}, u32[]{:S(2)}) async-start(bf16[16,80,128]{2,1,0:T(8,128)(2,1)} %shard_map.168), calls=%async_computation.6 | async-start | bytes 655360 | tf_op jit(solution)/shard_map/all_to_all | solution.py:308
  126.2 3.4 %collective-permute-start.5 = (bf16[80,512]{1,0:T(8,128)(2,1)S(1)}, bf16[80,512]{1,0:T(8,128)(2,1)S(1)}, u32[]{:S(2)}, u32[]{:S(2)}) collective-permute-start(bf16[80,512]{1,0:T(8,128)(2,1)S(1)} %get-tuple-element.62.h0), channel_id=1, source_target_pairs={{0,3},{1,0},{2,1},{3,2},{4,7},{5,4},{6,5},{7,6},{8,11},{9,8},{10,9... | collective-permute-start | bytes 245768 | tf_op jit(solution)/shard_map/ppermute | solution.py:312
  129.6 2.3 %collective-permute-start.4 = (bf16[80,512]{1,0:T(8,128)(2,1)S(1)}, bf16[80,512]{1,0:T(8,128)(2,1)S(1)}, u32[]{:S(2)}, u32[]{:S(2)}) collective-permute-start(bf16[80,512]{1,0:T(8,128)(2,1)S(1)} %get-tuple-element.62.h0), channel_id=1, source_target_pairs={{0,2},{1,3},{2,0},{3,1},{4,6},{5,7},{6,4},{7,5},{8,10},{9,11},{10,... | collective-permute-start | bytes 245768 | tf_op jit(solution)/shard_map/ppermute | solution.py:312
  131.9 4.1 %collective-permute-start.3 = (bf16[80,512]{1,0:T(8,128)(2,1)S(1)}, bf16[80,512]{1,0:T(8,128)(2,1)S(1)}, u32[]{:S(2)}, u32[]{:S(2)}) collective-permute-start(bf16[80,512]{1,0:T(8,128)(2,1)S(1)} %get-tuple-element.62.h0), channel_id=1, source_target_pairs={{0,1},{1,2},{2,3},{3,0},{4,5},{5,6},{6,7},{7,4},{8,9},{9,10},{10,1... | collective-permute-start | bytes 245768 | tf_op jit(solution)/shard_map/ppermute | solution.py:312
  136.1 1.7 %shard_map.170 = (f32[2,128,512]{2,1,0:T(8,128)}, f32[2,128,512]{2,1,0:T(8,128)}) custom-call(bf16[4,136,1024]{2,1,0:T(8,128)(2,1)S(1)} %all_to_all.38.main, bf16[512,256]{1,0:T(8,128)(2,1)S(1)} %bitcast.11), custom_call_target="tpu_custom_call" | custom-call | tf_op jit(solution)/shard_map/pallas_call | solution.py:49
  138.5 1.4 shard_map.171
  139.9 7.7 %all-to-all-done.6.got = bf16[16,80,128]{2,1,0:T(8,128)(2,1)S(1)} async-done(((bf16[16,80,128]{2,1,0:T(8,128)(2,1)}), bf16[16,80,128]{2,1,0:T(8,128)(2,1)S(1)}, u32[]{:S(2)}, u32[]{:S(2)}) %all-to-all-start.6) | async-done | bytes 327712 | tf_op jit(solution)/shard_map/all_to_all | solution.py:308
  147.6 0.9 shard_map.169
  (16 shorter events, 2.1 us)
Async XLA Ops:
  2.8 41.8 %all-to-all-start = ((bf16[32,16,256]{2,1,0:T(8,128)(2,1)}), bf16[32,16,256]{2,1,0:T(8,128)(2,1)S(1)}, u32[]{:S(2)}, u32[]{:S(2)}) async-start(bf16[32,16,256]{2,1,0:T(8,128)(2,1)} %bitcast.2), calls=%async_computation | async-start | bytes 524288 | tf_op jit(solution)/shard_map/all_to_all | solution.py:308
  22.3 9.9 %collective-permute-start.2 = (f16[32,1536]{1,0:T(8,128)(2,1)S(1)}, f16[32,1536]{1,0:T(8,128)(2,1)S(1)}, u32[]{:S(2)}, u32[]{:S(2)}) collective-permute-start(f16[32,1536]{1,0:T(8,128)(2,1)S(1)} %convert_element_type.34), channel_id=1, source_target_pairs={{0,2},{1,3},{2,0},{3,1},{4,6},{5,7},{6,4},{7,5},{8,10},{9,11},{10,... | collective-permute-start | bytes 294920 | tf_op jit(solution)/shard_map/ppermute | solution.py:312
  26.4 6.6 %collective-permute-start.1 = (f16[32,1536]{1,0:T(8,128)(2,1)S(1)}, f16[32,1536]{1,0:T(8,128)(2,1)S(1)}, u32[]{:S(2)}, u32[]{:S(2)}) collective-permute-start(f16[32,1536]{1,0:T(8,128)(2,1)S(1)} %convert_element_type.32), channel_id=1, source_target_pairs={{0,3},{1,0},{2,1},{3,2},{4,7},{5,4},{6,5},{7,6},{8,11},{9,8},{10,9... | collective-permute-start | bytes 294920 | tf_op jit(solution)/shard_map/ppermute | solution.py:312
  29.8 6.5 %collective-permute-start = (f16[32,1536]{1,0:T(8,128)(2,1)S(1)}, f16[32,1536]{1,0:T(8,128)(2,1)S(1)}, u32[]{:S(2)}, u32[]{:S(2)}) collective-permute-start(f16[32,1536]{1,0:T(8,128)(2,1)S(1)} %convert_element_type.30), channel_id=1, source_target_pairs={{0,1},{1,2},{2,3},{3,0},{4,5},{5,6},{6,7},{7,4},{8,9},{9,10},{10,1... | collective-permute-start | bytes 294920 | tf_op jit(solution)/shard_map/ppermute | solution.py:312
  121.3 26.3 %all-to-all-start.6 = ((bf16[16,80,128]{2,1,0:T(8,128)(2,1)}), bf16[16,80,128]{2,1,0:T(8,128)(2,1)S(1)}, u32[]{:S(2)}, u32[]{:S(2)}) async-start(bf16[16,80,128]{2,1,0:T(8,128)(2,1)} %shard_map.168), calls=%async_computation.6 | async-start | bytes 655360 | tf_op jit(solution)/shard_map/all_to_all | solution.py:308
  126.2 11.6 %collective-permute-start.5 = (bf16[80,512]{1,0:T(8,128)(2,1)S(1)}, bf16[80,512]{1,0:T(8,128)(2,1)S(1)}, u32[]{:S(2)}, u32[]{:S(2)}) collective-permute-start(bf16[80,512]{1,0:T(8,128)(2,1)S(1)} %get-tuple-element.62.h0), channel_id=1, source_target_pairs={{0,3},{1,0},{2,1},{3,2},{4,7},{5,4},{6,5},{7,6},{8,11},{9,8},{10,9... | collective-permute-start | bytes 245768 | tf_op jit(solution)/shard_map/ppermute | solution.py:312
  129.6 8.2 %collective-permute-start.4 = (bf16[80,512]{1,0:T(8,128)(2,1)S(1)}, bf16[80,512]{1,0:T(8,128)(2,1)S(1)}, u32[]{:S(2)}, u32[]{:S(2)}) collective-permute-start(bf16[80,512]{1,0:T(8,128)(2,1)S(1)} %get-tuple-element.62.h0), channel_id=1, source_target_pairs={{0,2},{1,3},{2,0},{3,1},{4,6},{5,7},{6,4},{7,5},{8,10},{9,11},{10,... | collective-permute-start | bytes 245768 | tf_op jit(solution)/shard_map/ppermute | solution.py:312
  131.9 6.6 %collective-permute-start.3 = (bf16[80,512]{1,0:T(8,128)(2,1)S(1)}, bf16[80,512]{1,0:T(8,128)(2,1)S(1)}, u32[]{:S(2)}, u32[]{:S(2)}) collective-permute-start(bf16[80,512]{1,0:T(8,128)(2,1)S(1)} %get-tuple-element.62.h0), channel_id=1, source_target_pairs={{0,1},{1,2},{2,3},{3,0},{4,5},{5,6},{6,7},{7,4},{8,9},{9,10},{10,1... | collective-permute-start | bytes 245768 | tf_op jit(solution)/shard_map/ppermute | solution.py:312
where the time goes:
time: 149 us
  blocking collectives  72.9 us (49%)
  starting transfers between devices  43.7 us (29%)
  waiting for transfers between devices  20.7 us (14%)
  Pallas kernels  10 us (7%)
    all_to_all x5, blocking collectives, swap(): return lax.all_to_all(array, axis, 0, 0, tiled=True)  72.9 us
    all_to_all x2, starting transfers between devices, swap(): return lax.all_to_all(array, axis, 0, 0, tiled=True)  24 us
    ppermute x6, starting transfers between devices, turn(): return lax.ppermute(array, 'x', [(i, (i + shift) % NX) for i in range(NX)])  19.7 us
    all_to_all x2, waiting for transfers between devices, swap(): return lax.all_to_all(array, axis, 0, 0, tiled=True)  16 us
    pallas_call x11, Pallas kernels, run(): pl.pallas_call(kernel, out_shape=outs, in_specs=[pl.BlockSpec(memory_spac...  10 us
    ppermute x6, waiting for transfers between devices, turn(): return lax.ppermute(array, 'x', [(i, (i + shift) % NX) for i in range(NX)])  4.7 us
  transfers between devices with their start and end apart: 8, of which 5 were waited for; matrix products, arithmetic and copies ran while one was open for 0% of the time, Pallas kernels for 2%

commit v1 on v0

--- a/solution.py
+++ b/solution.py
@@ -13,6 +13,7 @@
 SLOTS = 2 * CAP
 SHR = 4
 USED = SLOTS + SHR
+PACK = NC * (SLOTS + 2)
 HID = 512
 SCALE_X, SCALE_Y = 256.0, 64.0
 
@@ -204,7 +205,8 @@
     hid[...] = nn(onehot(y * BLK + q == iota((NY * SLOTS, NY * BLK), 1)), hidden).astype(BF)
 
 
-def back_kernel(main, tok, cot, wg, wu, sg, su, shared_grad, send):
+def back_kernel(main, tok, cot, wg, wu, sg, su, shared_grad, keep, send):
+    me = lax.axis_index("core")
     n = tok.shape[0]
     rows, total = NY * USED, NTP * USED
     grads = jnp.concatenate([main[x, :rows] for x in range(NX)], axis=0)
@@ -237,12 +239,14 @@
     back = back + nn(onehot((q == USED) & (source == lane)), lines[:, :128])
     back = back + nn(onehot((q == USED + 1) & (source == lane)), lines[:, 128:])
     back = back.astype(BF)
-    for d in range(NEP):
-        z, c = d // NC, d % NC
-        send[c, z, 0:BLK] = back[d * BLK : d * BLK + BLK]
-        send[c, z, BLK : 2 * BLK] = wt[d * BLK : d * BLK + BLK]
-        send[c, z, 2 * BLK : 3 * BLK] = wt[HID + d * BLK : HID + d * BLK + BLK]
-        send[c, z, 3 * BLK :] = wdn[d * BLK : d * BLK + BLK]
+    parts = (back, wt[:HID], wt[HID:], wdn)
+    for z in range(NZ):
+        for j, part in enumerate(parts):
+            a = part[2 * z * BLK : (2 * z + 1) * BLK]
+            b = part[(2 * z + 1) * BLK : (2 * z + 2) * BLK]
+            at = pl.ds(j * BLK, BLK)
+            keep[z, at] = jnp.where(me == 0, a, b)
+            send[z, at] = jnp.where(me == 0, b, a)
 
 
 def weights_kernel(main, recv, og, ou):
@@ -274,31 +278,37 @@
     od[0], od[1] = d[:, :128], d[:, 128:]
 
 
-def core_kernel(got, out):
+def core_kernel(kept, got, out):
+    me = lax.axis_index("core")
     for z in range(NZ):
-        out[z, :BLK] = got[0, z, :BLK]
-        out[z, BLK : 2 * BLK] = got[1, z, :BLK]
-        both = got[0, z, BLK:].astype(F32) + got[1, z, BLK:].astype(F32)
-        out[z, 2 * BLK :] = both.astype(BF)
+        mine, other = kept[z].astype(F32), got[z].astype(F32)
+        near, far = mine[:BLK], other[:BLK]
+        first, second = jnp.where(me == 0, near, far), jnp.where(me == 0, far, near)
+        out[z, :PACK] = jnp.concatenate(
+            [first[:SLOTS], second[:SLOTS], first[USED:], second[USED:]], axis=0
+        ).astype(BF)
+        out[z, PACK:] = (mine[BLK:] + other[BLK:]).astype(BF)
 
 
 def final_kernel(got, ids, shared_grad, grad_tokens, grad_weights, og, ou, od):
     n = ids.shape[1]
     row0, row1 = ids[0:1, :], ids[1:2, :]
-    back = jnp.concatenate([got[z, : 2 * BLK] for z in range(NZ)], axis=0)
-    tall = iota((NEP * BLK, n), 0)
-    places = onehot((row0 == tall) | (row1 == tall))
-    grad_tokens[...] = (tn(places, back) + shared_grad[...]).astype(BF)
+    back = jnp.concatenate([got[z, :PACK] for z in range(NZ)], axis=0)
+    tall = iota((NZ * PACK, n), 0)
     lane = iota((n, n), 0)
+    places = False
     for row, k in ((row0, 0), (row1, 1)):
-        base = (row >> 4) * BLK + USED
+        z, c, q = row >> 5, (row >> 4) & 1, row & 15
+        places = places | (z * PACK + c * SLOTS + q == tall)
+        base = z * PACK + NC * SLOTS + 2 * c
         line = tn(back, onehot((tall == base) | (tall == base + 1)))
         grad_weights[k : k + 1, :] = jnp.sum(
-            jnp.where(lane == (row & 15), line, 0.0), axis=0, keepdims=True
+            jnp.where(lane == q, line, 0.0), axis=0, keepdims=True
         )
-    total = got[0, 2 * BLK :].astype(F32)
+    grad_tokens[...] = (tn(onehot(places), back) + shared_grad[...]).astype(BF)
+    total = got[0, PACK:].astype(F32)
     for z in range(1, NZ):
-        total = total + got[z, 2 * BLK :].astype(F32)
+        total = total + got[z, PACK:].astype(F32)
     og[...] = total[:BLK]
     ou[...] = total[BLK : 2 * BLK]
     od[...] = total[2 * BLK :]
@@ -345,11 +355,10 @@
         pack_kernel, [((NX, NY * (BLK + 1), 2 * HID), BF), ((NY * SLOTS, HID), BF)]
     )(own)
     main = swap(main, "x")
-    shared_grad, back = call(
-        back_kernel, [((n, feats), F32), ((NC, NZ, 4 * BLK, feats), BF)]
-    )(main, tok, cot, wg, wu, sg, su)
-    back = swap(back, "core")
-    (back,) = call(core_kernel, [((NZ, 5 * BLK, feats), BF)])(back)
+    halves = ((NZ, 4 * BLK, feats), BF)
+    shared_grad, keep, give = call(back_kernel, [((n, feats), F32), halves, halves])(main, tok, cot, wg, wu, sg, su)
+    other = lax.ppermute(give, "core", [(0, 1), (1, 0)])
+    (back,) = call(core_kernel, [((NZ, PACK + 3 * BLK, feats), BF)])(keep, other)
     hid, back = lax.optimization_barrier((hid, back))
     turned = {k: turn(hid, k) for k in SHIFTS}
     back = swap(back, "z")

time: 149 us -> 147 us (0.987)
  blocking collectives: 72.9 us -> 68.7 us
  starting transfers between devices: 43.7 us -> 45.7 us
    all_to_all x5 -> x4, blocking collectives: 72.9 us -> 68.7 us  [swap(): return lax.all_to_all(array, axis, 0, 0, tiled=True)]
    ppermute x0 -> x1, starting transfers between devices: none -> 1.92 us  [body(): other = lax.ppermute(give, 'core', [(0, 1), (1, 0)])]
    ppermute x0 -> x1, waiting for transfers between devices: none -> 1.5 us  [body(): other = lax.ppermute(give, 'core', [(0, 1), (1, 0)])]
  transfers between devices with their start and end apart: 8 -> 9, of which waited for: 5 -> 6; matrix products, arithmetic and copies ran while one was open for 0% -> 0% of each run, Pallas kernels for 2% -> 2%
where the time goes in v1:
time: 147 us; the launch traced here: 146 us
  blocking collectives  68.7 us (47%)
  starting transfers between devices  45.7 us (31%)
  waiting for transfers between devices  20.7 us (14%)
  Pallas kernels  10 us (7%)
    all_to_all x4, blocking collectives, swap(): return lax.all_to_all(array, axis, 0, 0, tiled=True)  68.7 us
    all_to_all x2, starting transfers between devices, swap(): return lax.all_to_all(array, axis, 0, 0, tiled=True)  24 us
    ppermute x6, starting transfers between devices, turn(): return lax.ppermute(array, 'x', [(i, (i + shift) % NX) for i in range(NX)])  19.7 us
    all_to_all x2, waiting for transfers between devices, swap(): return lax.all_to_all(array, axis, 0, 0, tiled=True)  14.5 us
    pallas_call x11, Pallas kernels, run(): pl.pallas_call(kernel, out_shape=outs, in_specs=[pl.BlockSpec(memory_spac...  10 us
    ppermute x6, waiting for transfers between devices, turn(): return lax.ppermute(array, 'x', [(i, (i + shift) % NX) for i in range(NX)])  4.7 us
  transfers between devices with their start and end apart: 9, of which 6 were waited for; matrix products, arithmetic and copies ran while one was open for 0% of the time, Pallas kernels for 2%

profile of v1, /device:TPU:2, one launch (start us, length us, event | category | flops | bytes accessed | tf_op | source)
XLA Modules:
  0.0 146.3 jit_solution(1741959272429856151)
XLA Ops:
  0.6 2.1 %shard_map.161 = (bf16[512,256]{1,0:T(8,128)(2,1)}, s32[2,128]{1,0:T(2,128)S(1)}, bf16[128,128]{1,0:T(8,128)(2,1)S(1)}, bf16[128,128]{1,0:T(8,128)(2,1)S(1)}, bf...) custom-call(s32[2,128]{1,0:T(2,128)} %bitcast.16, ...), custom_call_target="tpu_custom_call" | custom-call | tf_op jit(solution)/shard_map/pallas_call | solution.py:50
  2.8 19.2 %all-to-all-start = ((bf16[32,16,256]{2,1,0:T(8,128)(2,1)}), bf16[32,16,256]{2,1,0:T(8,128)(2,1)S(1)}, u32[]{:S(2)}, u32[]{:S(2)}) async-start(bf16[32,16,256]{2,1,0:T(8,128)(2,1)} %bitcast.2), calls=%async_computation | async-start | bytes 524288 | tf_op jit(solution)/shard_map/all_to_all | solution.py:318
  22.3 4.0 %collective-permute-start.2 = (f16[32,1536]{1,0:T(8,128)(2,1)S(1)}, f16[32,1536]{1,0:T(8,128)(2,1)S(1)}, u32[]{:S(2)}, u32[]{:S(2)}) collective-permute-start(f16[32,1536]{1,0:T(8,128)(2,1)S(1)} %convert_element_type.34), channel_id=1, source_target_pairs={{0,2},{1,3},{2,0},{3,1},{4,6},{5,7},{6,4},{7,5},{8,10},{9,11},{10,... | collective-permute-start | bytes 294920 | tf_op jit(solution)/shard_map/ppermute | solution.py:322
  26.4 3.4 %collective-permute-start.1 = (f16[32,1536]{1,0:T(8,128)(2,1)S(1)}, f16[32,1536]{1,0:T(8,128)(2,1)S(1)}, u32[]{:S(2)}, u32[]{:S(2)}) collective-permute-start(f16[32,1536]{1,0:T(8,128)(2,1)S(1)} %convert_element_type.32), channel_id=1, source_target_pairs={{0,3},{1,0},{2,1},{3,2},{4,7},{5,4},{6,5},{7,6},{8,11},{9,8},{10,9... | collective-permute-start | bytes 294920 | tf_op jit(solution)/shard_map/ppermute | solution.py:322
  29.8 2.5 %collective-permute-start = (f16[32,1536]{1,0:T(8,128)(2,1)S(1)}, f16[32,1536]{1,0:T(8,128)(2,1)S(1)}, u32[]{:S(2)}, u32[]{:S(2)}) collective-permute-start(f16[32,1536]{1,0:T(8,128)(2,1)S(1)} %convert_element_type.30), channel_id=1, source_target_pairs={{0,1},{1,2},{2,3},{3,0},{4,5},{5,6},{6,7},{7,4},{8,9},{9,10},{10,1... | collective-permute-start | bytes 294920 | tf_op jit(solution)/shard_map/ppermute | solution.py:322
  33.0 3.3 %collective-permute-done = f16[32,1536]{1,0:T(8,128)(2,1)S(1)} collective-permute-done((f16[32,1536]{1,0:T(8,128)(2,1)S(1)}, f16[32,1536]{1,0:T(8,128)(2,1)S(1)}, u32[]{:S(2)}, u32[]{:S(2)}) %collective-permute-start) | collective-permute-done | bytes 98336 | tf_op jit(solution)/shard_map/ppermute | solution.py:322
  36.3 8.3 %all-to-all-done.recv = bf16[32,16,256]{2,1,0:T(8,128)(2,1)S(1)} async-done(((bf16[32,16,256]{2,1,0:T(8,128)(2,1)}), bf16[32,16,256]{2,1,0:T(8,128)(2,1)S(1)}, u32[]{:S(2)}, u32[]{:S(2)}) %all-to-all-start) | async-done | bytes 262176 | tf_op jit(solution)/shard_map/all_to_all | solution.py:318
  44.6 0.7 shard_map.163
  45.4 17.6 %all_to_all.30 = f16[4,80,1536]{2,1,0:T(8,128)(2,1)S(1)} all-to-all(f16[4,80,1536]{2,1,0:T(8,128)(2,1)S(1)} %bitcast.14), channel_id=1, replica_groups=mesh['z'=16,'core'=2,'y'=8,'x'=4] {'x'}, dimensions={0} | all-to-all | bytes 1966080 | tf_op jit(solution)/shard_map/all_to_all | solution.py:318
  63.4 20.5 %all_to_all.31 = f16[8,16,1536]{2,1,0:T(8,128)(2,1)S(1)} all-to-all(f16[8,16,1536]{2,1,0:T(8,128)(2,1)S(1)} %bitcast.15), channel_id=1, replica_groups=mesh['z'=16,'core'=2,'y'=8,'x'=4] {'y'}, dimensions={0} | all-to-all | bytes 786432 | tf_op jit(solution)/shard_map/all_to_all | solution.py:318
  84.0 15.5 %all_to_all.32 = bf16[8,16,1536]{2,1,0:T(8,128)(2,1)S(1)} all-to-all(bf16[8,16,1536]{2,1,0:T(8,128)(2,1)S(1)} %shard_map.165), channel_id=1, replica_groups=mesh['z'=16,'core'=2,'y'=8,'x'=4] {'y'}, dimensions={0} | all-to-all | bytes 786432 | tf_op jit(solution)/shard_map/all_to_all | solution.py:318
  99.9 15.1 %all_to_all.33.main = bf16[4,136,1024]{2,1,0:T(8,128)(2,1)S(1)} all-to-all(bf16[4,136,1024]{2,1,0:T(8,128)(2,1)S(1)} %get-tuple-element.54), channel_id=1, replica_groups=mesh['z'=16,'core'=2,'y'=8,'x'=4] {'x'}, dimensions={0} | all-to-all | bytes 2228224 | tf_op jit(solution)/shard_map/all_to_all | solution.py:318
  115.0 1.4 shard_map.167
  116.4 1.9 %collective-permute-start.3 = (bf16[16,64,128]{2,1,0:T(8,128)(2,1)S(1)}, bf16[16,64,128]{2,1,0:T(8,128)(2,1)S(1)}, u32[]{:S(2)}, u32[]{:S(2)}) collective-permute-start(bf16[16,64,128]{2,1,0:T(8,128)(2,1)S(1)} %get-tuple-element.56), channel_id=1, source_target_pairs={{0,32},{32,0},{1,33},{33,1},{2,34},{34,2},{3,35},{35,3},{4,36},{36... | collective-permute-start | bytes 786440 | tf_op jit(solution)/shard_map/ppermute | solution.py:360
  118.3 1.5 %collective-permute-done.3.got = bf16[16,64,128]{2,1,0:T(8,128)(2,1)S(1)} collective-permute-done((bf16[16,64,128]{2,1,0:T(8,128)(2,1)S(1)}, bf16[16,64,128]{2,1,0:T(8,128)(2,1)S(1)}, u32[]{:S(2)}, u32[]{:S(2)}) %collective-permute-start.3) | collective-permute-done | bytes 262176 | tf_op jit(solution)/shard_map/ppermute | solution.py:360
  119.8 0.8 shard_map.168
  120.6 4.9 %all-to-all-start.5 = ((bf16[16,72,128]{2,1,0:T(8,128)(2,1)}), bf16[16,72,128]{2,1,0:T(8,128)(2,1)S(1)}, u32[]{:S(2)}, u32[]{:S(2)}) async-start(bf16[16,72,128]{2,1,0:T(8,128)(2,1)} %shard_map.168), calls=%async_computation.5 | async-start | bytes 589824 | tf_op jit(solution)/shard_map/all_to_all | solution.py:318
  125.5 3.4 %collective-permute-start.6 = (bf16[80,512]{1,0:T(8,128)(2,1)S(1)}, bf16[80,512]{1,0:T(8,128)(2,1)S(1)}, u32[]{:S(2)}, u32[]{:S(2)}) collective-permute-start(bf16[80,512]{1,0:T(8,128)(2,1)S(1)} %get-tuple-element.64.h0), channel_id=1, source_target_pairs={{0,3},{1,0},{2,1},{3,2},{4,7},{5,4},{6,5},{7,6},{8,11},{9,8},{10,9... | collective-permute-start | bytes 245768 | tf_op jit(solution)/shard_map/ppermute | solution.py:322
  128.9 2.3 %collective-permute-start.5 = (bf16[80,512]{1,0:T(8,128)(2,1)S(1)}, bf16[80,512]{1,0:T(8,128)(2,1)S(1)}, u32[]{:S(2)}, u32[]{:S(2)}) collective-permute-start(bf16[80,512]{1,0:T(8,128)(2,1)S(1)} %get-tuple-element.64.h0), channel_id=1, source_target_pairs={{0,2},{1,3},{2,0},{3,1},{4,6},{5,7},{6,4},{7,5},{8,10},{9,11},{10,... | collective-permute-start | bytes 245768 | tf_op jit(solution)/shard_map/ppermute | solution.py:322
  131.2 4.1 %collective-permute-start.4 = (bf16[80,512]{1,0:T(8,128)(2,1)S(1)}, bf16[80,512]{1,0:T(8,128)(2,1)S(1)}, u32[]{:S(2)}, u32[]{:S(2)}) collective-permute-start(bf16[80,512]{1,0:T(8,128)(2,1)S(1)} %get-tuple-element.64.h0), channel_id=1, source_target_pairs={{0,1},{1,2},{2,3},{3,0},{4,5},{5,6},{6,7},{7,4},{8,9},{9,10},{10,1... | collective-permute-start | bytes 245768 | tf_op jit(solution)/shard_map/ppermute | solution.py:322
  135.4 1.7 %shard_map.170 = (f32[2,128,512]{2,1,0:T(8,128)}, f32[2,128,512]{2,1,0:T(8,128)}) custom-call(bf16[4,136,1024]{2,1,0:T(8,128)(2,1)S(1)} %all_to_all.33.main, bf16[512,256]{1,0:T(8,128)(2,1)S(1)} %bitcast.11), custom_call_target="tpu_custom_call" | custom-call | tf_op jit(solution)/shard_map/pallas_call | solution.py:50
  137.8 1.4 shard_map.171
  139.2 6.2 %all-to-all-done.5.got = bf16[16,72,128]{2,1,0:T(8,128)(2,1)S(1)} async-done(((bf16[16,72,128]{2,1,0:T(8,128)(2,1)}), bf16[16,72,128]{2,1,0:T(8,128)(2,1)S(1)}, u32[]{:S(2)}, u32[]{:S(2)}) %all-to-all-start.5) | async-done | bytes 294944 | tf_op jit(solution)/shard_map/all_to_all | solution.py:318
  145.4 0.9 shard_map.169
  (17 shorter events, 2.8 us)
Async XLA Ops:
  2.8 41.8 %all-to-all-start = ((bf16[32,16,256]{2,1,0:T(8,128)(2,1)}), bf16[32,16,256]{2,1,0:T(8,128)(2,1)S(1)}, u32[]{:S(2)}, u32[]{:S(2)}) async-start(bf16[32,16,256]{2,1,0:T(8,128)(2,1)} %bitcast.2), calls=%async_computation | async-start | bytes 524288 | tf_op jit(solution)/shard_map/all_to_all | solution.py:318
  22.3 9.9 %collective-permute-start.2 = (f16[32,1536]{1,0:T(8,128)(2,1)S(1)}, f16[32,1536]{1,0:T(8,128)(2,1)S(1)}, u32[]{:S(2)}, u32[]{:S(2)}) collective-permute-start(f16[32,1536]{1,0:T(8,128)(2,1)S(1)} %convert_element_type.34), channel_id=1, source_target_pairs={{0,2},{1,3},{2,0},{3,1},{4,6},{5,7},{6,4},{7,5},{8,10},{9,11},{10,... | collective-permute-start | bytes 294920 | tf_op jit(solution)/shard_map/ppermute | solution.py:322
  26.4 6.6 %collective-permute-start.1 = (f16[32,1536]{1,0:T(8,128)(2,1)S(1)}, f16[32,1536]{1,0:T(8,128)(2,1)S(1)}, u32[]{:S(2)}, u32[]{:S(2)}) collective-permute-start(f16[32,1536]{1,0:T(8,128)(2,1)S(1)} %convert_element_type.32), channel_id=1, source_target_pairs={{0,3},{1,0},{2,1},{3,2},{4,7},{5,4},{6,5},{7,6},{8,11},{9,8},{10,9... | collective-permute-start | bytes 294920 | tf_op jit(solution)/shard_map/ppermute | solution.py:322
  29.8 6.5 %collective-permute-start = (f16[32,1536]{1,0:T(8,128)(2,1)S(1)}, f16[32,1536]{1,0:T(8,128)(2,1)S(1)}, u32[]{:S(2)}, u32[]{:S(2)}) collective-permute-start(f16[32,1536]{1,0:T(8,128)(2,1)S(1)} %convert_element_type.30), channel_id=1, source_target_pairs={{0,1},{1,2},{2,3},{3,0},{4,5},{5,6},{6,7},{7,4},{8,9},{9,10},{10,1... | collective-permute-start | bytes 294920 | tf_op jit(solution)/shard_map/ppermute | solution.py:322
  116.4 3.4 %collective-permute-start.3 = (bf16[16,64,128]{2,1,0:T(8,128)(2,1)S(1)}, bf16[16,64,128]{2,1,0:T(8,128)(2,1)S(1)}, u32[]{:S(2)}, u32[]{:S(2)}) collective-permute-start(bf16[16,64,128]{2,1,0:T(8,128)(2,1)S(1)} %get-tuple-element.56), channel_id=1, source_target_pairs={{0,32},{32,0},{1,33},{33,1},{2,34},{34,2},{3,35},{35,3},{4,36},{36... | collective-permute-start | bytes 786440 | tf_op jit(solution)/shard_map/ppermute | solution.py:360
  120.6 24.8 %all-to-all-start.5 = ((bf16[16,72,128]{2,1,0:T(8,128)(2,1)}), bf16[16,72,128]{2,1,0:T(8,128)(2,1)S(1)}, u32[]{:S(2)}, u32[]{:S(2)}) async-start(bf16[16,72,128]{2,1,0:T(8,128)(2,1)} %shard_map.168), calls=%async_computation.5 | async-start | bytes 589824 | tf_op jit(solution)/shard_map/all_to_all | solution.py:318
  125.5 11.6 %collective-permute-start.6 = (bf16[80,512]{1,0:T(8,128)(2,1)S(1)}, bf16[80,512]{1,0:T(8,128)(2,1)S(1)}, u32[]{:S(2)}, u32[]{:S(2)}) collective-permute-start(bf16[80,512]{1,0:T(8,128)(2,1)S(1)} %get-tuple-element.64.h0), channel_id=1, source_target_pairs={{0,3},{1,0},{2,1},{3,2},{4,7},{5,4},{6,5},{7,6},{8,11},{9,8},{10,9... | collective-permute-start | bytes 245768 | tf_op jit(solution)/shard_map/ppermute | solution.py:322
  128.9 8.2 %collective-permute-start.5 = (bf16[80,512]{1,0:T(8,128)(2,1)S(1)}, bf16[80,512]{1,0:T(8,128)(2,1)S(1)}, u32[]{:S(2)}, u32[]{:S(2)}) collective-permute-start(bf16[80,512]{1,0:T(8,128)(2,1)S(1)} %get-tuple-element.64.h0), channel_id=1, source_target_pairs={{0,2},{1,3},{2,0},{3,1},{4,6},{5,7},{6,4},{7,5},{8,10},{9,11},{10,... | collective-permute-start | bytes 245768 | tf_op jit(solution)/shard_map/ppermute | solution.py:322
  131.2 6.6 %collective-permute-start.4 = (bf16[80,512]{1,0:T(8,128)(2,1)S(1)}, bf16[80,512]{1,0:T(8,128)(2,1)S(1)}, u32[]{:S(2)}, u32[]{:S(2)}) collective-permute-start(bf16[80,512]{1,0:T(8,128)(2,1)S(1)} %get-tuple-element.64.h0), channel_id=1, source_target_pairs={{0,1},{1,2},{2,3},{3,0},{4,5},{5,6},{6,7},{7,4},{8,9},{9,10},{10,1... | collective-permute-start | bytes 245768 | tf_op jit(solution)/shard_map/ppermute | solution.py:322
